TPU v7x, 32 devices: a whole 2x2x4 slice. The times are simulated.
32 devices in a mesh: ep: 16 (over z, y, x), tp: 2 (over core).
Axes of the slice: x: 2, y: 2, z: 4, core: 2. Of those that a mesh axis runs over, the one named last changes fastest.
Arguments:
- tokens: bfloat16 [256, 2048], P('ep', 'tp'), may hold values from -6 to 6
- state: float32 [256, 4, 128, 128], P('ep', 'tp'), may hold values from -4 to 4
- norm_mix: float32 [2048], replicated, may hold values from 0.1 to 1.9
- w_query: bfloat16 [2048, 512], P(None, 'tp'), may hold values from -0.125 to 0.125
- w_key: bfloat16 [2048, 512], P(None, 'tp'), may hold values from -0.125 to 0.125
- w_value: bfloat16 [2048, 512], P(None, 'tp'), may hold values from -0.125 to 0.125
- w_out: bfloat16 [512, 2048], P('tp'), may hold values from -0.25 to 0.25
- norm_ffn: float32 [2048], P('tp'), may hold values from 0.1 to 1.9
- gate_vector: bfloat16 [2048], P('tp'), may hold values from -0.125 to 0.125
- dense_gate: bfloat16 [2048, 2816], P('tp', 'ep'), may hold values from -0.125 to 0.125
- dense_up: bfloat16 [2048, 2816], P('tp', 'ep'), may hold values from -0.125 to 0.125
- dense_down: bfloat16 [2816, 2048], P('ep', 'tp'), may hold values from -0.109375 to 0.109375
- exp_gate: bfloat16 [16, 2048, 1408], P('ep', None, 'tp'), may hold values from -0.125 to 0.125
- exp_up: bfloat16 [16, 2048, 1408], P('ep', None, 'tp'), may hold values from -0.125 to 0.125
- exp_down: bfloat16 [16, 1408, 2048], P('ep', 'tp'), may hold values from -0.109375 to 0.109375
- routes: int32 [256, 2], P('ep'), may hold values from 0 to 7, all different within a row; in each aligned block of 16 rows (0 to 15, 16 to 31, ...) at most 5 rows name the same one
- route_w: bfloat16 [256, 2], P('ep'), may hold values from 0.099609375 to 1
Outputs:
- mixed: bfloat16 [256, 2048], P('ep', 'tp')
- new_state: float32 [256, 4, 128, 128], P('ep', 'tp')
Inputs may be any that keep to these rules, and one draw needn't show every extreme that they name: `routes`: each row names 2 different experts. Within the rows of one device (aligned blocks of 16 rows) no expert is named by more than 5 rows, a bound that some blocks reach.
All inputs are finite; a program needn't handle non-finite values.
Results may differ from a plain program's by a relative error of at most 0.014.
Values may be sent and summed in bfloat16 or wider, within the bound.
A program may use at most 128 MiB of HBM per device.

v0:
```python
import jax
import jax.numpy as jnp
from jax import lax
from jax.sharding import PartitionSpec as P

EXPERTS = 8
CAP = 5
epsilon = 1e-06


def route_tables(routes, route_w):
    onehot = (routes[:, :, None] == jnp.arange(EXPERTS, dtype=jnp.int32)[None, None, :]).astype(
        jnp.float32
    )
    member = jnp.sum(onehot, axis=1)
    weight = jnp.sum(onehot * route_w.astype(jnp.float32)[:, :, None], axis=1)
    place = jnp.cumsum(member, axis=0) - member
    slot_ids = jnp.arange(CAP, dtype=jnp.float32)
    select = member.T[:, None, :] * (place.T[:, None, :] == slot_ids[None, :, None]).astype(
        jnp.float32
    )
    return (select, weight)


def expert_math(flat_rows, weights):
    gate_pre = jnp.dot(flat_rows, weights[0], preferred_element_type=jnp.float32)
    up_part = jnp.dot(flat_rows, weights[1], preferred_element_type=jnp.float32)
    hidden = (jax.nn.silu(gate_pre) * up_part).astype(jnp.bfloat16)
    return jnp.dot(hidden, weights[2], preferred_element_type=jnp.float32)


def expert_apply(slot_rows, weights):
    full_rows = lax.all_gather(slot_rows, "tp", axis=2, tiled=True)
    row_count = full_rows.shape[0] * full_rows.shape[1]
    partial_value = expert_math(full_rows.reshape(row_count, full_rows.shape[2]), weights)
    summed = lax.psum_scatter(
        partial_value.astype(jnp.bfloat16), "tp", scatter_dimension=1, tiled=True
    ).astype(jnp.float32)
    return summed.reshape(slot_rows.shape[0], slot_rows.shape[1], summed.shape[1])


def body(
    tokens,
    state,
    norm_mix,
    w_query,
    w_key,
    w_value,
    w_out,
    norm_ffn,
    gate_vector,
    dense_gate,
    dense_up,
    dense_down,
    exp_gate,
    exp_up,
    exp_down,
    routes,
    route_w,
):
    highest = lax.Precision.HIGHEST
    row_count, half_width = tokens.shape
    heads_here, head_size = (state.shape[1], state.shape[2])
    weights = (exp_gate[0], exp_up[0], exp_down[0])
    full_x = lax.all_gather(tokens, "tp", axis=1, tiled=True)
    width = full_x.shape[1]
    full_f = full_x.astype(jnp.float32)
    normed = (
        full_f
        * lax.rsqrt(jnp.sum(full_f * full_f, axis=1, keepdims=True) / width + epsilon)
        * norm_mix
    ).astype(jnp.bfloat16)
    query = jnp.dot(normed, w_query, preferred_element_type=jnp.float32).astype(jnp.bfloat16)
    key_rows = jnp.dot(normed, w_key, preferred_element_type=jnp.float32).astype(jnp.bfloat16)
    value_rows = jnp.dot(normed, w_value, preferred_element_type=jnp.float32).astype(jnp.bfloat16)
    query3 = query.astype(jnp.float32).reshape(row_count, heads_here, head_size)
    key3 = key_rows.astype(jnp.float32).reshape(row_count, heads_here, head_size) * head_size ** (
        -0.5
    )
    value3 = value_rows.astype(jnp.float32).reshape(row_count, heads_here, head_size)
    head_ids = (lax.axis_index("tp") * heads_here + jnp.arange(heads_here, dtype=jnp.int32)).astype(
        jnp.float32
    )
    decay = 1.0 - jnp.exp2(-3.0 - 2.0 * head_ids)
    new_state = decay[None, :, None, None] * state + jnp.einsum(
        "shd,she->shde", key3, value3, precision=highest
    )
    read = jnp.einsum("shd,shde->she", query3, new_state, precision=highest)
    centre = jnp.mean(read, axis=2, keepdims=True)
    spread = jnp.mean(jnp.square(read - centre), axis=2, keepdims=True)
    heads_out = (
        ((read - centre) * lax.rsqrt(spread + epsilon))
        .astype(jnp.bfloat16)
        .reshape(row_count, heads_here * head_size)
    )
    mix_part = jnp.dot(heads_out, w_out, preferred_element_type=jnp.float32)
    mix_half = lax.psum_scatter(
        mix_part.astype(jnp.bfloat16), "tp", scatter_dimension=1, tiled=True
    ).astype(jnp.float32)
    after = (tokens.astype(jnp.float32) + mix_half).astype(jnp.bfloat16)
    after_hf = after.astype(jnp.float32)
    squares = lax.psum(jnp.sum(after_hf * after_hf, axis=1, keepdims=True), "tp")
    after_f = after.astype(jnp.float32)
    normed2 = (after_f * lax.rsqrt(squares / width + epsilon) * norm_ffn).astype(jnp.bfloat16)
    all_rows = lax.all_gather(normed2, "ep", axis=0, tiled=True)
    dense_pre = jnp.dot(all_rows, dense_gate, preferred_element_type=jnp.float32)
    up_pre = jnp.dot(all_rows, dense_up, preferred_element_type=jnp.float32)
    logit = jnp.dot(all_rows, gate_vector, preferred_element_type=jnp.float32)
    dense_pre, up_pre, logit = (
        lax.psum(dense_pre.astype(jnp.bfloat16), "tp").astype(jnp.float32),
        lax.psum(up_pre.astype(jnp.bfloat16), "tp").astype(jnp.float32),
        lax.psum(logit.astype(jnp.bfloat16), "tp").astype(jnp.float32),
    )
    dense_hidden = (jax.nn.sigmoid(logit)[:, None] * jax.nn.silu(dense_pre) * up_pre).astype(
        jnp.bfloat16
    )
    ep_count = lax.axis_size("ep")
    group_size = ep_count // EXPERTS
    select, weight = route_tables(routes, route_w)
    outgoing = jnp.einsum(
        "ecr,rd->ecd", select.astype(jnp.bfloat16), normed2, preferred_element_type=jnp.float32
    ).astype(jnp.bfloat16)
    outgoing = jnp.repeat(outgoing, group_size, axis=0)
    served = expert_apply(
        lax.all_to_all(outgoing, "ep", split_axis=0, concat_axis=0, tiled=True), weights
    )
    returned = lax.all_to_all(
        served.astype(jnp.bfloat16), "ep", split_axis=0, concat_axis=0, tiled=True
    ).astype(served.dtype)
    per_expert = jnp.sum(returned.reshape(EXPERTS, group_size, CAP, half_width), axis=1)
    local_moe = jnp.einsum(
        "ecr,ecd->rd", select * weight.T[:, None, :], per_expert, precision=highest
    )
    value = jnp.dot(dense_hidden, dense_down, preferred_element_type=jnp.float32)
    combined = lax.psum_scatter(value, "ep", scatter_dimension=0, tiled=True)
    return ((after_f + local_moe + combined).astype(jnp.bfloat16), new_state)


def solution(mesh):
    return jax.shard_map(
        body,
        mesh=mesh,
        in_specs=(
            P("ep", "tp"),
            P("ep", "tp", None, None),
            P(),
            P(None, "tp"),
            P(None, "tp"),
            P(None, "tp"),
            P("tp", None),
            P("tp"),
            P("tp"),
            P("tp", "ep"),
            P("tp", "ep"),
            P("ep", "tp"),
            P("ep", None, "tp"),
            P("ep", None, "tp"),
            P("ep", "tp", None),
            P("ep", None),
            P("ep", None),
        ),
        out_specs=(P("ep", "tp"), P("ep", "tp", None, None)),
        check_vma=False,
    )
```

profile of v0, /device:TPU:0, one launch (start us, length us, event | category | flops | bytes accessed | tf_op | source)
XLA Modules:
  0.0 210.0 jit_solution(15320848404340629431)
XLA Ops:
  7.2 2.3 %all_gather.9 = bf16[16,2048]{1,0:T(8,128)(2,1)S(1)} all-gather(bf16[16,1024]{1,0:T(8,128)(2,1)} %param.17), channel_id=1, replica_groups=mesh['ep'=16,'tp'=2] {'tp'}, dimensions={1}, use_global_device_ids=true | all-gather | bytes 98304 | tf_op jit(solution)/shard_map/all_gather | solution.py:65
  9.7 1.5 convolution_convert_fusion.6
  11.3 1.5 fusion.18
  12.8 1.5 fusion.20
  14.4 2.0 multiply_add_fusion
  16.4 1.3 copy-done.1
  17.7 1.1 fusion.63
  18.9 0.2 multiply_reduce_fusion
  19.2 2.1 convolution_convert_fusion
  21.6 10.0 %reduce-scatter.4.cloned.1.call-done = bf16[16,1024]{1,0:T(8,128)(2,1)} async-done(((bf16[16,2048]{1,0:T(8,128)(2,1)}), bf16[16,1024]{1,0:T(8,128)(2,1)}) %reduce-scatter.4.cloned.1.call-update) | async-done | bytes 32784 | tf_op jit(solution)/shard_map/reduce_scatter | solution.py:97
  31.6 0.9 fusion.43
  32.5 2.5 %psum.28 = f32[16,1]{0,1:T(1,128)S(1)} all-reduce(f32[16,1]{0,1:T(1,128)S(1)} %bitcast.72), channel_id=1, replica_groups=mesh['ep'=16,'tp'=2] {'tp'}, use_global_device_ids=true, to_apply=%region_8.0 | all-reduce | flops 16 | bytes 128 | tf_op jit(solution)/shard_map/psum | solution.py:102
  35.0 0.8 fusion.45
  35.8 44.0 %all_gather.11 = bf16[256,1024]{1,0:T(8,128)(2,1)S(1)} all-gather(bf16[16,1024]{1,0:T(8,128)(2,1)S(1)} %fusion.45), channel_id=1, replica_groups=mesh['ep'=16,'tp'=2] {'ep'}, dimensions={0}, use_global_device_ids=true | all-gather | bytes 557056 | tf_op jit(solution)/shard_map/all_gather | solution.py:105
  79.8 0.1 convolution_convert_fusion.3
  80.0 0.7 broadcast_in_dim.5
  80.7 4.2 %all-to-all-start = ((bf16[16,5,1024]{2,1,0:T(8,128)(2,1)}), bf16[16,5,1024]{2,1,0:T(8,128)(2,1)}, u32[]{:S(2)}, u32[]{:S(2)}) async-start(bf16[16,5,1024]{2,1,0:T(8,128)(2,1)} %bitcast.63), calls=%async_computation.1 | async-start | bytes 524288 | tf_op jit(solution)/shard_map/all_to_all | solution.py:125
  84.9 1.9 convolution_convert_fusion.1
  86.9 2.0 convolution_convert_fusion.2
  88.9 4.5 %all-to-all-done = bf16[16,5,1024]{2,1,0:T(8,128)(2,1)} async-done(((bf16[16,5,1024]{2,1,0:T(8,128)(2,1)}), bf16[16,5,1024]{2,1,0:T(8,128)(2,1)}, u32[]{:S(2)}, u32[]{:S(2)}) %all-to-all-start) | async-done | bytes 163872 | tf_op jit(solution)/shard_map/all_to_all | solution.py:125
  93.4 3.8 %all_gather.10 = bf16[16,5,2048]{2,1,0:T(8,128)(2,1)} all-gather(bf16[16,5,1024]{2,1,0:T(8,128)(2,1)} %all-to-all-done), channel_id=1, replica_groups=mesh['ep'=16,'tp'=2] {'tp'}, dimensions={2}, use_global_device_ids=true | all-gather | bytes 491520 | tf_op jit(solution)/shard_map/all_gather | solution.py:33
  97.2 1.9 reshape.74
  99.1 3.6 %fusion.4 = f32[80,704]{1,0:T(8,128)} fusion(bf16[80,2048]{1,0:T(8,128)(2,1)} %reshape.74, bf16[1,2048,704]{1,2,0:T(8,128)(2,1)} %param.29), kind=kOutput, calls=%fused_computation.4 | convolution fusion | flops 230686720 | bytes 3436544 | tf_op jit(solution)/shard_map/dot_general | solution.py:26
  102.7 4.5 %fusion.6 = bf16[80,2048]{1,0:T(8,128)(2,1)} fusion(bf16[1,704,2048]{2,1,0:T(8,128)(2,1)S(1)} %copy-done, bf16[80,2048]{1,0:T(8,128)(2,1)} %reshape.74, bf16[1,2048,704]{1,2,0:T(8,128)(2,1)} %param.30, f32[80,704]{1,0:T(8,128)} %fusion.4), kind=kOutput, calls=%fused_computation.6 | convolution fusion | flops 461875200 | bytes 6647808 | tf_op jit(solution)/shard_map/dot_general | solution.py:29
  107.3 0.2 fusion.64
  107.6 2.5 %psum.29 = bf16[256]{0:T(256)(128)(2,1)S(1)} all-reduce(bf16[256]{0:T(256)(128)(2,1)S(1)} %convert_element_type.119), channel_id=1, replica_groups=mesh['ep'=16,'tp'=2] {'tp'}, use_global_device_ids=true, to_apply=%region_11.12 | all-reduce | flops 256 | bytes 1024 | tf_op jit(solution)/shard_map/psum | solution.py:112
  110.1 2.4 %fusion.39 = f32[256,1024]{1,0:T(8,128)} fusion(bf16[176,1024]{1,0:T(8,128)(2,1)} %param.28, bf16[256,176]{0,1:T(8,128)(2,1)} %get-tuple-element.4, bf16[256,176]{0,1:T(8,128)(2,1)} %get-tuple-element.5, f32[256]{0:T(256)S(1)} %add_divide_fusion), kind=kOutput, calls=%fused_computation.47 | convolution fusion | flops 92680192 | bytes 1590272 | tf_op jit(solution)/shard_map/dot_general | solution.py:134
  112.5 7.0 %reduce-scatter.6.cloned.1.call-done = bf16[80,1024]{1,0:T(8,128)(2,1)} async-done(((bf16[80,2048]{1,0:T(8,128)(2,1)}), bf16[80,1024]{1,0:T(8,128)(2,1)}) %reduce-scatter.6.cloned.1.call-update) | async-done | bytes 163856 | tf_op jit(solution)/shard_map/reduce_scatter | solution.py:36
  119.6 1.0 convert_element_type.118
  120.6 18.1 %all_to_all.10 = bf16[16,5,1024]{2,1,0:T(8,128)(2,1)S(1)} all-to-all(bf16[16,5,1024]{2,1,0:T(8,128)(2,1)S(1)} %convert_element_type.118), channel_id=1, replica_groups=mesh['ep'=16,'tp'=2] {'ep'}, dimensions={0} | all-to-all | bytes 327680 | tf_op jit(solution)/shard_map/all_to_all | solution.py:127
  138.8 63.0 %reduce-scatter.8.cloned.1.call-done = f32[16,1024]{1,0:T(8,128)} async-done(((f32[256,1024]{1,0:T(8,128)}), f32[16,1024]{1,0:T(8,128)}) %reduce-scatter.8.cloned.1.call-update) | async-done | bytes 65552 | tf_op jit(solution)/shard_map/reduce_scatter | solution.py:135
  201.7 1.8 fusion.17
  (46 shorter events, 1.0 us)
Async XLA Ops:
  7.2 95.6 %copy-start = (bf16[1,704,2048]{2,1,0:T(8,128)(2,1)S(1)}, bf16[1,704,2048]{2,1,0:T(8,128)(2,1)}, u32[]{:S(2)}) copy-start(bf16[1,704,2048]{2,1,0:T(8,128)(2,1)} %param.31) | copy-start | bytes 8650756
  7.2 24.4 %reduce-scatter.4.cloned.1.call-start = ((), (), s32[]{:S(2)}) async-start(), calls=%async_computation.5 | async-start | bytes 98304 | tf_op jit(solution)/shard_map/reduce_scatter | solution.py:97
  14.4 6.9 %copy-start.5 = (bf16[1024]{0:T(1024)(128)(2,1)S(1)}, bf16[1024]{0:T(1024)(128)(2,1)}, u32[]{:S(2)}) copy-start(bf16[1024]{0:T(1024)(128)(2,1)} %param.25) | copy-start | bytes 6148
  14.4 7.0 %copy-start.7 = (bf16[16,2]{0,1:T(2,128)(2,1)S(1)}, bf16[16,2]{0,1:T(2,128)(2,1)}, u32[]{:S(2)}) copy-start(bf16[16,2]{0,1:T(2,128)(2,1)} %param.33) | copy-start | bytes 196
  14.4 7.0 %copy-start.6 = (s32[16,2]{0,1:T(2,128)S(1)}, s32[16,2]{0,1:T(2,128)}, u32[]{:S(2)}) copy-start(s32[16,2]{0,1:T(2,128)} %param.32) | copy-start | bytes 388
  14.4 17.2 %copy-start.2 = (bf16[16,1024]{1,0:T(8,128)(2,1)S(1)}, bf16[16,1024]{1,0:T(8,128)(2,1)}, u32[]{:S(2)}) copy-start(bf16[16,1024]{1,0:T(8,128)(2,1)} %param.17) | copy-start | bytes 98308
  14.4 20.5 %copy-start.4 = (f32[1024]{0:T(1024)S(1)}, f32[1024]{0:T(1024)}, u32[]{:S(2)}) copy-start(f32[1024]{0:T(1024)} %param.24) | copy-start | bytes 12292
  16.4 1.3 copy-start.1
  80.7 12.7 %all-to-all-start = ((bf16[16,5,1024]{2,1,0:T(8,128)(2,1)}), bf16[16,5,1024]{2,1,0:T(8,128)(2,1)}, u32[]{:S(2)}, u32[]{:S(2)}) async-start(bf16[16,5,1024]{2,1,0:T(8,128)(2,1)} %bitcast.63), calls=%async_computation.1 | async-start | bytes 524288 | tf_op jit(solution)/shard_map/all_to_all | solution.py:125
  84.9 25.2 %all-reduce.3.cloned.1.call-start = ((), (), s32[]{:S(2)}) async-start(), calls=%async_computation.8 | async-start | bytes 360448 | tf_op jit(solution)/shard_map/psum | solution.py:111
  88.9 30.7 %reduce-scatter.6.cloned.1.call-start = ((), (), s32[]{:S(2)}) async-start(), calls=%async_computation.6 | async-start | bytes 491520 | tf_op jit(solution)/shard_map/reduce_scatter | solution.py:36
  107.2 94.5 %copy-start.3 = (bf16[16,1024]{1,0:T(8,128)(2,1)S(1)}, bf16[16,1024]{1,0:T(8,128)(2,1)}, u32[]{:S(2)}) copy-start(bf16[16,1024]{1,0:T(8,128)(2,1)} %reduce-scatter.4.cloned.1.call-done) | copy-start | bytes 98308
  107.3 94.4 %reduce-scatter.8.cloned.1.call-start = ((), (), s32[]{:S(2)}) async-start(), calls=%async_computation.7 | async-start | bytes 1114112 | tf_op jit(solution)/shard_map/reduce_scatter | solution.py:135
Sparse Core Ops, SparseCore 0:
  21.4 10.1 reduce-scatter.3
  89.0 19.2 all-reduce.2
  110.6 8.9 reduce-scatter.5
  121.7 79.9 reduce-scatter.7
where the time goes:
time: 211 us; the launch traced here: 210 us
  waiting for transfers between devices  84.5 us (40%)
  blocking collectives  73.3 us (35%)
  matrix products  24.3 us (12%)
  between operations  14 us (7%)
  local copies, waits for them, and re-layouts  5.22 us (2%)
  starting transfers between devices  4.35 us (2%)
  other arithmetic  4.33 us (2%)
    reduce_scatter x1, waiting for transfers between devices, body(): combined = lax.psum_scatter(value, 'ep', scatter_dimension=0, tiled=True)  63 us
    all_gather x1, blocking collectives, body(): all_rows = lax.all_gather(normed2, 'ep', axis=0, tiled=True)  44 us
    all_to_all x1, blocking collectives, body(): lax.all_to_all(served.astype(jnp.bfloat16), 'ep', split_axis=0, concat_ax...  18.1 us
    reduce_scatter x1, waiting for transfers between devices, body(): lax.psum_scatter(mix_part.astype(jnp.bfloat16), 'tp', scatter_dimension=1...  10 us
    reduce_scatter x1, waiting for transfers between devices, expert_apply(): lax.psum_scatter(partial_value.astype(jnp.bfloat16), 'tp', scatter_dimens...  7.02 us
    dot_general x1, matrix products, expert_math(): return jnp.dot(hidden, weights[2], preferred_element_type=jnp.float32)  4.51 us
    all_to_all x1, waiting for transfers between devices, body(): lax.all_to_all(outgoing, 'ep', split_axis=0, concat_axis=0, tiled=True)  4.47 us
  transfers between devices with their start and end apart: 5, of which 4 were waited for; matrix products, arithmetic and copies ran while one was open for 8% of the time, Pallas kernels for 0%

commit v1 on v0

--- a/solution.py
+++ b/solution.py
@@ -6,6 +6,16 @@
 EXPERTS = 8
 CAP = 5
 epsilon = 1e-06
+
+
+def turned_line(x, axis, dim):
+    count = lax.axis_size(axis)
+    held, shards = (x, [x])
+    for _ in range(count - 1):
+        held = lax.ppermute(held, axis, [(i, (i + 1) % count) for i in range(count)])
+        shards.insert(0, held)
+    row_of_blocks = jnp.concatenate(shards, axis=dim)
+    return jnp.roll(row_of_blocks, (lax.axis_index(axis) + 1) * x.shape[dim], axis=dim)
 
 
 def route_tables(routes, route_w):
@@ -102,7 +112,7 @@
     squares = lax.psum(jnp.sum(after_hf * after_hf, axis=1, keepdims=True), "tp")
     after_f = after.astype(jnp.float32)
     normed2 = (after_f * lax.rsqrt(squares / width + epsilon) * norm_ffn).astype(jnp.bfloat16)
-    all_rows = lax.all_gather(normed2, "ep", axis=0, tiled=True)
+    all_rows = turned_line(normed2, "ep", 0)
     dense_pre = jnp.dot(all_rows, dense_gate, preferred_element_type=jnp.float32)
     up_pre = jnp.dot(all_rows, dense_up, preferred_element_type=jnp.float32)
     logit = jnp.dot(all_rows, gate_vector, preferred_element_type=jnp.float32)

time: 211 us -> 278 us (1.32)
  waiting for transfers between devices: 84.5 us -> 185 us
  blocking collectives: 73.3 us -> 27.7 us
  starting transfers between devices: 4.35 us -> 11 us
  local copies, waits for them, and re-layouts: 5.22 us -> 10.6 us
    ppermute x0 -> x15, waiting for transfers between devices: none -> 96.7 us  [turned_line(): lax.ppermute(held, axis, [(i, (i + 1) % count) for i in range(count)])]
    all_gather x1 -> x0, blocking collectives: 44 us -> none  [body(): all_rows = lax.all_gather(normed2, 'ep', axis=0, tiled=True)]
    psum x1, waiting for transfers between devices: 0.01 us -> 6.51 us  [body(): lax.psum(up_pre.astype(jnp.bfloat16), 'tp').astype(jnp.float32)]
    unnamed x17 -> x106, local copies, waits for them, and re-layouts: 1.36 us -> 7.5 us
    all_to_all x1, waiting for transfers between devices: 4.47 us -> 0.01 us  [body(): lax.all_to_all(outgoing, 'ep', split_axis=0, concat_axis=0, tiled=True)]
    ppermute x0 -> x15, starting transfers between devices: none -> 3.79 us  [turned_line(): lax.ppermute(held, axis, [(i, (i + 1) % count) for i in range(count)])]
    all_to_all x1, starting transfers between devices: 4.19 us -> 7.01 us  [body(): lax.all_to_all(outgoing, 'ep', split_axis=0, concat_axis=0, tiled=True)]
  transfers between devices with their start and end apart: 5 -> 20, of which waited for: 4 -> 18; matrix products, arithmetic and copies ran while one was open for 8% -> 6% of each run, Pallas kernels for 0% -> 0%
where the time goes in v1:
time: 278 us; the launch traced here: 277 us
  waiting for transfers between devices  185 us (67%)
  blocking collectives  27.7 us (10%)
  matrix products  22.6 us (8%)
  between operations  14.4 us (5%)
  starting transfers between devices  11 us (4%)
  local copies, waits for them, and re-layouts  10.6 us (4%)
  other arithmetic  4.9 us (2%)
    ppermute x15, waiting for transfers between devices, turned_line(): lax.ppermute(held, axis, [(i, (i + 1) % count) for i in range(count)])  96.7 us
    reduce_scatter x1, waiting for transfers between devices, body(): combined = lax.psum_scatter(value, 'ep', scatter_dimension=0, tiled=True)  63 us
    all_to_all x1, blocking collectives, body(): lax.all_to_all(served.astype(jnp.bfloat16), 'ep', split_axis=0, concat_ax...  18.1 us
    reduce_scatter x1, waiting for transfers between devices, body(): lax.psum_scatter(mix_part.astype(jnp.bfloat16), 'tp', scatter_dimension=1...  10.3 us
    reduce_scatter x1, waiting for transfers between devices, expert_apply(): lax.psum_scatter(partial_value.astype(jnp.bfloat16), 'tp', scatter_dimens...  8.79 us
    unnamed x106, local copies, waits for them, and re-layouts  7.5 us
    all_to_all x1, starting transfers between devices, body(): lax.all_to_all(outgoing, 'ep', split_axis=0, concat_axis=0, tiled=True)  7.01 us
    psum x1, waiting for transfers between devices, body(): lax.psum(up_pre.astype(jnp.bfloat16), 'tp').astype(jnp.float32)  6.51 us
  transfers between devices with their start and end apart: 20, of which 18 were waited for; matrix products, arithmetic and copies ran while one was open for 6% of the time, Pallas kernels for 0%

profile of v1, /device:TPU:0, one launch (start us, length us, event | category | flops | bytes accessed | tf_op | source)
XLA Modules:
  0.0 276.5 jit_solution(7475546766716763805)
XLA Ops:
  7.2 2.3 all_gather.6
  14.4 2.0 multiply_add_fusion
  19.2 2.1 convolution_convert_fusion
  21.3 10.3 %reduce-scatter.4.cloned.1.call-done = bf16[16,1024]{1,0:T(8,128)(2,1)} async-done(((bf16[16,2048]{1,0:T(8,128)(2,1)}), bf16[16,1024]{1,0:T(8,128)(2,1)}) %reduce-scatter.4.cloned.1.call-update) | async-done | bytes 32784 | tf_op jit(solution)/shard_map/reduce_scatter | solution.py:107
  32.5 2.5 psum.28
  35.8 1.7 collective-permute-start
  37.5 5.8 %collective-permute-done = bf16[16,1024]{1,0:T(8,128)(2,1)S(1)} collective-permute-done((bf16[16,1024]{1,0:T(8,128)(2,1)S(1)}, bf16[16,1024]{1,0:T(8,128)(2,1)S(1)}, u32[]{:S(2)}, u32[]{:S(2)}) %collective-permute-start) | collective-permute-done | bytes 32800 | tf_op jit(solution)/shard_map/ppermute | solution.py:15
  44.0 6.8 %collective-permute-done.1 = bf16[16,1024]{1,0:T(8,128)(2,1)S(1)} collective-permute-done((bf16[16,1024]{1,0:T(8,128)(2,1)S(1)}, bf16[16,1024]{1,0:T(8,128)(2,1)S(1)}, u32[]{:S(2)}, u32[]{:S(2)}) %collective-permute-start.1) | collective-permute-done | bytes 32800 | tf_op jit(solution)/shard_map/ppermute | solution.py:15
  50.9 7.4 %collective-permute-done.2 = bf16[16,1024]{1,0:T(8,128)(2,1)S(1)} collective-permute-done((bf16[16,1024]{1,0:T(8,128)(2,1)S(1)}, bf16[16,1024]{1,0:T(8,128)(2,1)S(1)}, u32[]{:S(2)}, u32[]{:S(2)}) %collective-permute-start.2) | collective-permute-done | bytes 32800 | tf_op jit(solution)/shard_map/ppermute | solution.py:15
  59.3 7.0 %all-to-all-start = ((bf16[16,5,1024]{2,1,0:T(8,128)(2,1)}), bf16[16,5,1024]{2,1,0:T(8,128)(2,1)S(1)}, u32[]{:S(2)}, u32[]{:S(2)}) async-start(bf16[16,5,1024]{2,1,0:T(8,128)(2,1)} %bitcast.9), calls=%async_computation.1 | async-start | bytes 524288 | tf_op jit(solution)/shard_map/all_to_all | solution.py:135
  66.4 2.0 collective-permute-start.4
  68.3 7.7 %collective-permute-done.4 = bf16[16,1024]{1,0:T(8,128)(2,1)S(1)} collective-permute-done((bf16[16,1024]{1,0:T(8,128)(2,1)S(1)}, bf16[16,1024]{1,0:T(8,128)(2,1)S(1)}, u32[]{:S(2)}, u32[]{:S(2)}) %collective-permute-start.4) | collective-permute-done | bytes 32800 | tf_op jit(solution)/shard_map/ppermute | solution.py:15
  76.0 7.5 %collective-permute-done.5 = bf16[16,1024]{1,0:T(8,128)(2,1)S(1)} collective-permute-done((bf16[16,1024]{1,0:T(8,128)(2,1)S(1)}, bf16[16,1024]{1,0:T(8,128)(2,1)S(1)}, u32[]{:S(2)}, u32[]{:S(2)}) %collective-permute-start.5) | collective-permute-done | bytes 32800 | tf_op jit(solution)/shard_map/ppermute | solution.py:15
  83.5 7.5 %collective-permute-done.6 = bf16[16,1024]{1,0:T(8,128)(2,1)S(1)} collective-permute-done((bf16[16,1024]{1,0:T(8,128)(2,1)S(1)}, bf16[16,1024]{1,0:T(8,128)(2,1)S(1)}, u32[]{:S(2)}, u32[]{:S(2)}) %collective-permute-start.6) | collective-permute-done | bytes 32800 | tf_op jit(solution)/shard_map/ppermute | solution.py:15
  91.1 7.5 %collective-permute-done.7 = bf16[16,1024]{1,0:T(8,128)(2,1)S(1)} collective-permute-done((bf16[16,1024]{1,0:T(8,128)(2,1)S(1)}, bf16[16,1024]{1,0:T(8,128)(2,1)S(1)}, u32[]{:S(2)}, u32[]{:S(2)}) %collective-permute-start.7) | collective-permute-done | bytes 32800 | tf_op jit(solution)/shard_map/ppermute | solution.py:15
  98.6 7.5 %collective-permute-done.8 = bf16[16,1024]{1,0:T(8,128)(2,1)S(1)} collective-permute-done((bf16[16,1024]{1,0:T(8,128)(2,1)S(1)}, bf16[16,1024]{1,0:T(8,128)(2,1)S(1)}, u32[]{:S(2)}, u32[]{:S(2)}) %collective-permute-start.8) | collective-permute-done | bytes 32800 | tf_op jit(solution)/shard_map/ppermute | solution.py:15
  106.1 7.5 %collective-permute-done.9 = bf16[16,1024]{1,0:T(8,128)(2,1)S(1)} collective-permute-done((bf16[16,1024]{1,0:T(8,128)(2,1)S(1)}, bf16[16,1024]{1,0:T(8,128)(2,1)S(1)}, u32[]{:S(2)}, u32[]{:S(2)}) %collective-permute-start.9) | collective-permute-done | bytes 32800 | tf_op jit(solution)/shard_map/ppermute | solution.py:15
  113.6 7.5 %collective-permute-done.10 = bf16[16,1024]{1,0:T(8,128)(2,1)S(1)} collective-permute-done((bf16[16,1024]{1,0:T(8,128)(2,1)S(1)}, bf16[16,1024]{1,0:T(8,128)(2,1)S(1)}, u32[]{:S(2)}, u32[]{:S(2)}) %collective-permute-start.10) | collective-permute-done | bytes 32800 | tf_op jit(solution)/shard_map/ppermute | solution.py:15
  121.1 7.6 %collective-permute-done.11 = bf16[16,1024]{1,0:T(8,128)(2,1)} collective-permute-done((bf16[16,1024]{1,0:T(8,128)(2,1)S(1)}, bf16[16,1024]{1,0:T(8,128)(2,1)}, u32[]{:S(2)}, u32[]{:S(2)}) %collective-permute-start.11) | collective-permute-done | bytes 32800 | tf_op jit(solution)/shard_map/ppermute | solution.py:15
  129.3 7.2 %collective-permute-done.12 = bf16[16,1024]{1,0:T(8,128)(2,1)} collective-permute-done((bf16[16,1024]{1,0:T(8,128)(2,1)}, bf16[16,1024]{1,0:T(8,128)(2,1)}, u32[]{:S(2)}, u32[]{:S(2)}) %collective-permute-start.12) | collective-permute-done | bytes 32800 | tf_op jit(solution)/shard_map/ppermute | solution.py:15
  136.6 2.3 all_gather.7
  140.1 4.2 %collective-permute-done.13 = bf16[16,1024]{1,0:T(8,128)(2,1)} collective-permute-done((bf16[16,1024]{1,0:T(8,128)(2,1)}, bf16[16,1024]{1,0:T(8,128)(2,1)}, u32[]{:S(2)}, u32[]{:S(2)}) %collective-permute-start.13) | collective-permute-done | bytes 32800 | tf_op jit(solution)/shard_map/ppermute | solution.py:15
  144.6 2.8 %fusion.4 = f32[80,704]{1,0:T(8,128)S(1)} fusion(bf16[80,2048]{1,0:T(8,128)(2,1)S(1)} %reshape.74, bf16[1,2048,704]{1,2,0:T(8,128)(2,1)} %param.29), kind=kOutput, calls=%fused_computation.4 | convolution fusion | flops 230686720 | bytes 3436544 | tf_op jit(solution)/shard_map/dot_general | solution.py:36
  147.4 4.8 %collective-permute-done.14 = bf16[16,1024]{1,0:T(8,128)(2,1)S(1)} collective-permute-done((bf16[16,1024]{1,0:T(8,128)(2,1)}, bf16[16,1024]{1,0:T(8,128)(2,1)S(1)}, u32[]{:S(2)}, u32[]{:S(2)}) %collective-permute-start.14) | collective-permute-done | bytes 32800 | tf_op jit(solution)/shard_map/ppermute | solution.py:15
  160.0 4.4 %fusion.6 = bf16[80,2048]{1,0:T(8,128)(2,1)} fusion(bf16[1,704,2048]{2,1,0:T(8,128)(2,1)S(1)} %copy-done, bf16[80,2048]{1,0:T(8,128)(2,1)S(1)} %reshape.74, bf16[1,2048,704]{1,2,0:T(8,128)(2,1)} %param.30, f32[80,704]{1,0:T(8,128)S(1)} %fusion.4), kind=kOutput, calls=%fused_computation.6 | convolution fusion | flops 461875200 | bytes 6647808 | tf_op jit(solution)/shard_map/dot_general | solution.py:39
  165.8 2.4 psum.29
  168.3 6.5 %all-reduce.3.cloned.1.call-done = (bf16[256,176]{0,1:T(8,128)(2,1)}, bf16[256,176]{0,1:T(8,128)(2,1)}) async-done(((bf16[256,176]{0,1:T(8,128)(2,1)}, bf16[256,176]{0,1:T(8,128)(2,1)}), (bf16[256,176]{0,1:T(8,128)(2,1)}, bf16[256,176]{0,1:T(8,128)(2,1)})) %all-reduce.3.cloned.1.call-update) | async-done | bytes 180240 | tf_op jit(solution)/shard_map/psum | solution.py:121
  174.8 2.4 fusion.43
  177.3 8.8 %reduce-scatter.6.cloned.1.call-done = bf16[80,1024]{1,0:T(8,128)(2,1)} async-done(((bf16[80,2048]{1,0:T(8,128)(2,1)}), bf16[80,1024]{1,0:T(8,128)(2,1)}) %reduce-scatter.6.cloned.1.call-update) | async-done | bytes 163856 | tf_op jit(solution)/shard_map/reduce_scatter | solution.py:46
  187.0 18.1 %all_to_all.10 = bf16[16,5,1024]{2,1,0:T(8,128)(2,1)S(1)} all-to-all(bf16[16,5,1024]{2,1,0:T(8,128)(2,1)S(1)} %convert_element_type.118), channel_id=1, replica_groups=mesh['ep'=16,'tp'=2] {'ep'}, dimensions={0} | all-to-all | bytes 327680 | tf_op jit(solution)/shard_map/all_to_all | solution.py:137
  205.2 63.0 %reduce-scatter.8.cloned.1.call-done = f32[16,1024]{1,0:T(8,128)} async-done(((f32[256,1024]{1,0:T(8,128)}), f32[16,1024]{1,0:T(8,128)}) %reduce-scatter.8.cloned.1.call-update) | async-done | bytes 65552 | tf_op jit(solution)/shard_map/reduce_scatter | solution.py:145
  268.3 1.8 fusion.17
  (165 shorter events, 23.0 us)
Async XLA Ops:
  7.2 152.9 %copy-start = (bf16[1,704,2048]{2,1,0:T(8,128)(2,1)S(1)}, bf16[1,704,2048]{2,1,0:T(8,128)(2,1)}, u32[]{:S(2)}) copy-start(bf16[1,704,2048]{2,1,0:T(8,128)(2,1)} %param.31) | copy-start | bytes 8650756
  7.2 24.4 %reduce-scatter.4.cloned.1.call-start = ((), (), s32[]{:S(2)}) async-start(), calls=%async_computation.5 | async-start | bytes 98304 | tf_op jit(solution)/shard_map/reduce_scatter | solution.py:107
  17.7 111.0 %copy-start.34 = (bf16[1024]{0:T(1024)(128)(2,1)S(1)}, bf16[1024]{0:T(1024)(128)(2,1)}, u32[]{:S(2)}) copy-start(bf16[1024]{0:T(1024)(128)(2,1)} %param.25) | copy-start | bytes 6148
  35.8 7.5 %collective-permute-start = (bf16[16,1024]{1,0:T(8,128)(2,1)S(1)}, bf16[16,1024]{1,0:T(8,128)(2,1)S(1)}, u32[]{:S(2)}, u32[]{:S(2)}) collective-permute-start(bf16[16,1024]{1,0:T(8,128)(2,1)S(1)} %fusion.49), channel_id=1, source_target_pairs={{0,2},{2,4},{4,6},{6,8},{8,10},{10,12},{12,14},{14,16},{16,18},{18... | collective-permute-start | bytes 98312 | tf_op jit(solution)/shard_map/ppermute | solution.py:15
  43.3 7.5 %collective-permute-start.1 = (bf16[16,1024]{1,0:T(8,128)(2,1)S(1)}, bf16[16,1024]{1,0:T(8,128)(2,1)S(1)}, u32[]{:S(2)}, u32[]{:S(2)}) collective-permute-start(bf16[16,1024]{1,0:T(8,128)(2,1)S(1)} %collective-permute-done), channel_id=1, source_target_pairs={{0,2},{2,4},{4,6},{6,8},{8,10},{10,12},{12,14},{14,16},{16,18},{18... | collective-permute-start | bytes 98312 | tf_op jit(solution)/shard_map/ppermute | solution.py:15
  50.8 7.5 %collective-permute-start.2 = (bf16[16,1024]{1,0:T(8,128)(2,1)S(1)}, bf16[16,1024]{1,0:T(8,128)(2,1)S(1)}, u32[]{:S(2)}, u32[]{:S(2)}) collective-permute-start(bf16[16,1024]{1,0:T(8,128)(2,1)S(1)} %collective-permute-done.1), channel_id=1, source_target_pairs={{0,2},{2,4},{4,6},{6,8},{8,10},{10,12},{12,14},{14,16},{16,18},{18... | collective-permute-start | bytes 98312 | tf_op jit(solution)/shard_map/ppermute | solution.py:15
  58.3 78.2 %copy-start.9 = (bf16[16,1024]{1,0:T(8,128)(2,1)}, bf16[16,1024]{1,0:T(8,128)(2,1)S(1)}, u32[]{:S(2)}) copy-start(bf16[16,1024]{1,0:T(8,128)(2,1)S(1)} %collective-permute-done.2) | copy-start | bytes 98308
  58.3 8.0 %collective-permute-start.3 = (bf16[16,1024]{1,0:T(8,128)(2,1)S(1)}, bf16[16,1024]{1,0:T(8,128)(2,1)S(1)}, u32[]{:S(2)}, u32[]{:S(2)}) collective-permute-start(bf16[16,1024]{1,0:T(8,128)(2,1)S(1)} %collective-permute-done.2), channel_id=1, source_target_pairs={{0,2},{2,4},{4,6},{6,8},{8,10},{10,12},{12,14},{14,16},{16,18},{18... | collective-permute-start | bytes 98312 | tf_op jit(solution)/shard_map/ppermute | solution.py:15
  59.3 77.3 %all-to-all-start = ((bf16[16,5,1024]{2,1,0:T(8,128)(2,1)}), bf16[16,5,1024]{2,1,0:T(8,128)(2,1)S(1)}, u32[]{:S(2)}, u32[]{:S(2)}) async-start(bf16[16,5,1024]{2,1,0:T(8,128)(2,1)} %bitcast.9), calls=%async_computation.1 | async-start | bytes 524288 | tf_op jit(solution)/shard_map/all_to_all | solution.py:135
  66.3 108.5 %all-reduce.3.cloned.1.call-start = ((), (), s32[]{:S(2)}) async-start(), calls=%async_computation.8 | async-start | bytes 360448 | tf_op jit(solution)/shard_map/psum | solution.py:121
  66.4 70.2 %copy-start.11 = (bf16[16,1024]{1,0:T(8,128)(2,1)}, bf16[16,1024]{1,0:T(8,128)(2,1)S(1)}, u32[]{:S(2)}) copy-start(bf16[16,1024]{1,0:T(8,128)(2,1)S(1)} %collective-permute-done.3) | copy-start | bytes 98308
  66.4 9.7 %collective-permute-start.4 = (bf16[16,1024]{1,0:T(8,128)(2,1)S(1)}, bf16[16,1024]{1,0:T(8,128)(2,1)S(1)}, u32[]{:S(2)}, u32[]{:S(2)}) collective-permute-start(bf16[16,1024]{1,0:T(8,128)(2,1)S(1)} %collective-permute-done.3), channel_id=1, source_target_pairs={{0,2},{2,4},{4,6},{6,8},{8,10},{10,12},{12,14},{14,16},{16,18},{18... | collective-permute-start | bytes 98312 | tf_op jit(solution)/shard_map/ppermute | solution.py:15
  76.0 68.4 %copy-start.13 = (bf16[16,1024]{1,0:T(8,128)(2,1)}, bf16[16,1024]{1,0:T(8,128)(2,1)S(1)}, u32[]{:S(2)}) copy-start(bf16[16,1024]{1,0:T(8,128)(2,1)S(1)} %collective-permute-done.4) | copy-start | bytes 98308
  76.0 7.5 %collective-permute-start.5 = (bf16[16,1024]{1,0:T(8,128)(2,1)S(1)}, bf16[16,1024]{1,0:T(8,128)(2,1)S(1)}, u32[]{:S(2)}, u32[]{:S(2)}) collective-permute-start(bf16[16,1024]{1,0:T(8,128)(2,1)S(1)} %collective-permute-done.4), channel_id=1, source_target_pairs={{0,2},{2,4},{4,6},{6,8},{8,10},{10,12},{12,14},{14,16},{16,18},{18... | collective-permute-start | bytes 98312 | tf_op jit(solution)/shard_map/ppermute | solution.py:15
  83.5 60.8 %copy-start.15 = (bf16[16,1024]{1,0:T(8,128)(2,1)}, bf16[16,1024]{1,0:T(8,128)(2,1)S(1)}, u32[]{:S(2)}) copy-start(bf16[16,1024]{1,0:T(8,128)(2,1)S(1)} %collective-permute-done.5) | copy-start | bytes 98308
  83.5 7.5 %collective-permute-start.6 = (bf16[16,1024]{1,0:T(8,128)(2,1)S(1)}, bf16[16,1024]{1,0:T(8,128)(2,1)S(1)}, u32[]{:S(2)}, u32[]{:S(2)}) collective-permute-start(bf16[16,1024]{1,0:T(8,128)(2,1)S(1)} %collective-permute-done.5), channel_id=1, source_target_pairs={{0,2},{2,4},{4,6},{6,8},{8,10},{10,12},{12,14},{14,16},{16,18},{18... | collective-permute-start | bytes 98312 | tf_op jit(solution)/shard_map/ppermute | solution.py:15
  91.1 53.3 %copy-start.17 = (bf16[16,1024]{1,0:T(8,128)(2,1)}, bf16[16,1024]{1,0:T(8,128)(2,1)S(1)}, u32[]{:S(2)}) copy-start(bf16[16,1024]{1,0:T(8,128)(2,1)S(1)} %collective-permute-done.6) | copy-start | bytes 98308
  91.1 7.5 %collective-permute-start.7 = (bf16[16,1024]{1,0:T(8,128)(2,1)S(1)}, bf16[16,1024]{1,0:T(8,128)(2,1)S(1)}, u32[]{:S(2)}, u32[]{:S(2)}) collective-permute-start(bf16[16,1024]{1,0:T(8,128)(2,1)S(1)} %collective-permute-done.6), channel_id=1, source_target_pairs={{0,2},{2,4},{4,6},{6,8},{8,10},{10,12},{12,14},{14,16},{16,18},{18... | collective-permute-start | bytes 98312 | tf_op jit(solution)/shard_map/ppermute | solution.py:15
  98.6 45.8 %copy-start.19 = (bf16[16,1024]{1,0:T(8,128)(2,1)}, bf16[16,1024]{1,0:T(8,128)(2,1)S(1)}, u32[]{:S(2)}) copy-start(bf16[16,1024]{1,0:T(8,128)(2,1)S(1)} %collective-permute-done.7) | copy-start | bytes 98308
  98.6 7.5 %collective-permute-start.8 = (bf16[16,1024]{1,0:T(8,128)(2,1)S(1)}, bf16[16,1024]{1,0:T(8,128)(2,1)S(1)}, u32[]{:S(2)}, u32[]{:S(2)}) collective-permute-start(bf16[16,1024]{1,0:T(8,128)(2,1)S(1)} %collective-permute-done.7), channel_id=1, source_target_pairs={{0,2},{2,4},{4,6},{6,8},{8,10},{10,12},{12,14},{14,16},{16,18},{18... | collective-permute-start | bytes 98312 | tf_op jit(solution)/shard_map/ppermute | solution.py:15
  106.1 7.5 %collective-permute-start.9 = (bf16[16,1024]{1,0:T(8,128)(2,1)S(1)}, bf16[16,1024]{1,0:T(8,128)(2,1)S(1)}, u32[]{:S(2)}, u32[]{:S(2)}) collective-permute-start(bf16[16,1024]{1,0:T(8,128)(2,1)S(1)} %collective-permute-done.8), channel_id=1, source_target_pairs={{0,2},{2,4},{4,6},{6,8},{8,10},{10,12},{12,14},{14,16},{16,18},{18... | collective-permute-start | bytes 98312 | tf_op jit(solution)/shard_map/ppermute | solution.py:15
  113.6 7.5 %collective-permute-start.10 = (bf16[16,1024]{1,0:T(8,128)(2,1)S(1)}, bf16[16,1024]{1,0:T(8,128)(2,1)S(1)}, u32[]{:S(2)}, u32[]{:S(2)}) collective-permute-start(bf16[16,1024]{1,0:T(8,128)(2,1)S(1)} %collective-permute-done.9), channel_id=1, source_target_pairs={{0,2},{2,4},{4,6},{6,8},{8,10},{10,12},{12,14},{14,16},{16,18},{18... | collective-permute-start | bytes 98312 | tf_op jit(solution)/shard_map/ppermute | solution.py:15
  121.1 7.6 %collective-permute-start.11 = (bf16[16,1024]{1,0:T(8,128)(2,1)S(1)}, bf16[16,1024]{1,0:T(8,128)(2,1)}, u32[]{:S(2)}, u32[]{:S(2)}) collective-permute-start(bf16[16,1024]{1,0:T(8,128)(2,1)S(1)} %collective-permute-done.10), channel_id=1, source_target_pairs={{0,2},{2,4},{4,6},{6,8},{8,10},{10,12},{12,14},{14,16},{16,18},{18... | collective-permute-start | bytes 98312 | tf_op jit(solution)/shard_map/ppermute | solution.py:15
  128.7 7.8 %collective-permute-start.12 = (bf16[16,1024]{1,0:T(8,128)(2,1)}, bf16[16,1024]{1,0:T(8,128)(2,1)}, u32[]{:S(2)}, u32[]{:S(2)}) collective-permute-start(bf16[16,1024]{1,0:T(8,128)(2,1)} %collective-permute-done.11), channel_id=1, source_target_pairs={{0,2},{2,4},{4,6},{6,8},{8,10},{10,12},{12,14},{14,16},{16,18},{18... | collective-permute-start | bytes 98312 | tf_op jit(solution)/shard_map/ppermute | solution.py:15
  136.6 7.8 %collective-permute-start.13 = (bf16[16,1024]{1,0:T(8,128)(2,1)}, bf16[16,1024]{1,0:T(8,128)(2,1)}, u32[]{:S(2)}, u32[]{:S(2)}) collective-permute-start(bf16[16,1024]{1,0:T(8,128)(2,1)} %collective-permute-done.12), channel_id=1, source_target_pairs={{0,2},{2,4},{4,6},{6,8},{8,10},{10,12},{12,14},{14,16},{16,18},{18... | collective-permute-start | bytes 98312 | tf_op jit(solution)/shard_map/ppermute | solution.py:15
  144.4 7.8 %collective-permute-start.14 = (bf16[16,1024]{1,0:T(8,128)(2,1)}, bf16[16,1024]{1,0:T(8,128)(2,1)S(1)}, u32[]{:S(2)}, u32[]{:S(2)}) collective-permute-start(bf16[16,1024]{1,0:T(8,128)(2,1)} %collective-permute-done.13), channel_id=1, source_target_pairs={{0,2},{2,4},{4,6},{6,8},{8,10},{10,12},{12,14},{14,16},{16,18},{18... | collective-permute-start | bytes 98312 | tf_op jit(solution)/shard_map/ppermute | solution.py:15
  160.0 26.1 %reduce-scatter.6.cloned.1.call-start = ((), (), s32[]{:S(2)}) async-start(), calls=%async_computation.6 | async-start | bytes 491520 | tf_op jit(solution)/shard_map/reduce_scatter | solution.py:46
  164.4 103.8 %copy-start.6 = (bf16[16,1024]{1,0:T(8,128)(2,1)S(1)}, bf16[16,1024]{1,0:T(8,128)(2,1)}, u32[]{:S(2)}) copy-start(bf16[16,1024]{1,0:T(8,128)(2,1)} %reduce-scatter.4.cloned.1.call-done) | copy-start | bytes 98308
  164.4 103.8 %copy-start.28 = (f32[16,8]{0,1:T(8,128)S(1)}, f32[16,8]{0,1:T(8,128)}, u32[]{:S(2)}) copy-start(f32[16,8]{0,1:T(8,128)} %copy-done.27) | copy-start | bytes 1540
  164.4 103.8 %copy-start.30 = (f32[8,16]{1,0:T(8,128)S(1)}, f32[8,16]{1,0:T(8,128)}, u32[]{:S(2)}) copy-start(f32[8,16]{1,0:T(8,128)} %copy-done.29) | copy-start | bytes 1540
  164.4 103.8 %copy-start.31 = (f32[16,8]{0,1:T(8,128)S(1)}, f32[16,8]{0,1:T(8,128)}, u32[]{:S(2)}) copy-start(f32[16,8]{0,1:T(8,128)} %get-tuple-element.2) | copy-start | bytes 1540
  164.5 103.8 %reduce-scatter.8.cloned.1.call-start = ((), (), s32[]{:S(2)}) async-start(), calls=%async_computation.7 | async-start | bytes 1114112 | tf_op jit(solution)/shard_map/reduce_scatter | solution.py:145
  (25 other events, 375.0 us)
Sparse Core Ops, SparseCore 0:
  21.4 10.1 reduce-scatter.3
  160.1 14.6 all-reduce.2
  177.0 8.9 reduce-scatter.5
  188.2 80.0 reduce-scatter.7
